TPU v7x, 32 devices: a whole 2x2x4 slice. The times are simulated.
32 devices in a mesh: rep: 2 (over x), fs: 4 (over z), tp: 4 (over y, core).
Axes of the slice: x: 2, y: 2, z: 4, core: 2. Of those that a mesh axis runs over, the one named last changes fastest.
Arguments:
- tokens: bfloat16 [8192, 1024], P(('rep', 'fs', 'tp')), may hold values from -6 to 6
- norm_gain: float32 [1024], replicated, may hold values from 0.5 to 1.5
- gate_weight: bfloat16 [1024, 3072], P(('rep', 'fs'), 'tp'), may hold values from -0.1875 to 0.1875
- up_weight: bfloat16 [1024, 3072], P(('rep', 'fs'), 'tp'), may hold values from -0.1875 to 0.1875
- down_weight: bfloat16 [3072, 1024], P('tp', ('rep', 'fs')), may hold values from -0.109375 to 0.109375
Outputs:
- block_out: bfloat16 [8192, 1024], P(('rep', 'fs', 'tp'))
All inputs are finite; a program needn't handle non-finite values.
Results may differ from a plain program's by a relative error of at most 0.001.
Values may be sent and summed in bfloat16 or wider, within the bound.
A program may use at most 64 MiB of HBM per device.

v0:
```python
import jax
import jax.numpy as jnp
from jax import lax
from jax.sharding import PartitionSpec as P

epsilon = 1e-06


def over_all(shard, axis, dim, absorb, carry):
    whole = jax.tree.map(lambda part: lax.all_gather(part, axis, axis=dim, tiled=True), shard)
    return absorb(carry, whole, jnp.int32(0))


def summed_rows(portion, width, axis):
    count = width * lax.axis_size(axis)
    return lax.psum_scatter(portion(jnp.int32(0), count), axis, scatter_dimension=0, tiled=True)


def on_device(tokens, norm_gain, gate_weight, up_weight, down_weight):
    values = tokens.astype(jnp.float32)
    inverse_rms = lax.rsqrt(jnp.mean(values * values, axis=-1, keepdims=True) + epsilon)
    normed = (values * inverse_rms * norm_gain.astype(jnp.float32)).astype(jnp.bfloat16)
    gathered = lax.all_gather(normed, "tp", axis=0, tiled=True)
    zero_sums = jnp.zeros((gathered.shape[0], gate_weight.shape[1]), jnp.float32)

    def add_block(running, row_block, first_row):
        columns = lax.dynamic_slice_in_dim(gathered, first_row, row_block.shape[0], 1)
        return running + jnp.dot(columns, row_block, preferred_element_type=jnp.float32)

    gate_value = over_all(gate_weight, ("rep", "fs"), 0, add_block, zero_sums)
    up_value = over_all(up_weight, ("rep", "fs"), 0, add_block, zero_sums)
    hidden = (jax.nn.silu(gate_value) * up_value).astype(jnp.bfloat16)
    own_half = lax.all_gather(down_weight, "fs", axis=1, tiled=True)
    down_whole = lax.all_gather(own_half, "rep", axis=1, tiled=True)
    own_rows = tokens.shape[0]

    def row_terms(first_row, row_count):
        token_block = lax.dynamic_slice_in_dim(hidden, first_row, row_count, 0)
        return jnp.dot(token_block, down_whole, preferred_element_type=jnp.float32)

    mixed_out = summed_rows(row_terms, own_rows, "tp")
    return mixed_out.astype(jnp.bfloat16)


def solution(mesh):
    return jax.shard_map(
        on_device,
        mesh=mesh,
        in_specs=(
            P(("rep", "fs", "tp"), None),
            P(),
            P(("rep", "fs"), "tp"),
            P(("rep", "fs"), "tp"),
            P("tp", ("rep", "fs")),
        ),
        out_specs=P(("rep", "fs", "tp"), None),
        check_vma=False,
    )
```

profile of v0, /device:TPU:0, one launch (start us, length us, event | category | flops | bytes accessed | tf_op | source)
XLA Modules:
  0.0 218.2 jit_solution(9125715528160293608)
XLA Ops:
  6.5 0.0 copy-start
  6.5 0.0 all-gather.7.cloned.1.call-start
  6.5 0.7 all-gather.7.cloned.1.call-update
  7.3 0.0 all-gather.5.cloned.1.call-start
  7.3 1.2 fusion.1
  8.5 2.0 fusion.3
  10.6 0.0 all-gather.5.cloned.1.call-update
  10.6 0.0 all-gather.11.cloned.1.call-start
  10.6 0.0 copy-done
  10.7 26.2 %all_gather.18 = bf16[768,512]{1,0:T(8,128)(2,1)} all-gather(bf16[768,128]{1,0:T(8,128)(2,1)S(1)} %copy-done), channel_id=1, replica_groups=mesh['rep'=2,'fs'=4,'tp'=4] {'fs'}, dimensions={1}, use_global_device_ids=true | all-gather | bytes 983040 | tf_op jit(solution)/shard_map/all_gather | solution.py:33
  36.8 0.0 all-gather.11.cloned.1.call-update
  36.9 0.0 all-gather.9.cloned.1.call-start
  36.9 0.5 all-gather.9.cloned.1.call-update
  37.5 0.0 reduce-scatter.2.cloned.1.call-start
  37.5 22.4 %all-gather.7.cloned.1.call-done = bf16[1024,768]{1,0:T(8,128)(2,1)} async-done(((bf16[128,768]{1,0:T(8,128)(2,1)}), bf16[1024,768]{1,0:T(8,128)(2,1)}) %all-gather.7.cloned.1.call-update) | async-done | bytes 1572880 | tf_op jit(solution)/shard_map/all_gather | solution.py:10
  59.9 22.5 %all-gather.5.cloned.1.call-done = bf16[1024,1024]{1,0:T(8,128)(2,1)} async-done(((bf16[256,1024]{1,0:T(8,128)(2,1)}), bf16[1024,1024]{1,0:T(8,128)(2,1)}) %all-gather.5.cloned.1.call-update) | async-done | bytes 2097168 | tf_op jit(solution)/shard_map/all_gather | solution.py:23
  82.4 0.0 copy-start.1
  82.4 5.6 %fusion.5 = f32[1024,768]{1,0:T(8,128)} fusion(bf16[1024,1024]{1,0:T(8,128)(2,1)} %all-gather.5.cloned.1.call-done, bf16[1024,768]{1,0:T(8,128)(2,1)} %all-gather.7.cloned.1.call-done), kind=kOutput, calls=%fused_computation.9 | convolution fusion | flops 1610612736 | bytes 6815744 | tf_op jit(solution)/shard_map/dot_general | solution.py:28
  88.0 23.1 %all-gather.11.cloned.1.call-done = bf16[768,1024]{1,0:T(8,128)(2,1)} async-done(((bf16[768,512]{1,0:T(8,128)(2,1)}), bf16[768,1024]{1,0:T(8,128)(2,1)}) %all-gather.11.cloned.1.call-update) | async-done | bytes 1572880 | tf_op jit(solution)/shard_map/all_gather | solution.py:34
  111.2 46.2 %all-gather.9.cloned.1.call-done = bf16[1024,768]{1,0:T(8,128)(2,1)} async-done(((bf16[128,768]{1,0:T(8,128)(2,1)}), bf16[1024,768]{1,0:T(8,128)(2,1)}) %all-gather.9.cloned.1.call-update) | async-done | bytes 1572880 | tf_op jit(solution)/shard_map/all_gather | solution.py:10
  157.3 0.0 copy-done.1
  157.3 9.1 %fusion = f32[1024,1024]{1,0:T(8,128)} fusion(bf16[768,1024]{1,0:T(8,128)(2,1)} %all-gather.11.cloned.1.call-done, f32[1024,768]{1,0:T(8,128)} %fusion.5, bf16[1024,1024]{1,0:T(8,128)(2,1)S(1)} %copy-done.1, bf16[1024,768]{1,0:T(8,128)(2,1)} %all-gather.9.cloned.1.call-done), kind=kOutput, calls=%fused_computation.1 | convolution fusion | flops 3225944064 | bytes 12582912 | tf_op jit(solution)/shard_map/dot_general | solution.py:39
  166.5 0.0 reduce-scatter.2.cloned.1.call-update
  166.5 43.1 %reduce-scatter.2.cloned.1.call-done = f32[256,1024]{1,0:T(8,128)} async-done(((f32[1024,1024]{1,0:T(8,128)}), f32[256,1024]{1,0:T(8,128)}) %reduce-scatter.2.cloned.1.call-update) | async-done | bytes 1048592 | tf_op jit(solution)/shard_map/reduce_scatter | solution.py:16
  209.6 2.1 convert_element_type.15
  (1 shorter events, 0.0 us)
Async XLA Ops:
  6.5 4.1 %copy-start = (bf16[768,128]{1,0:T(8,128)(2,1)S(1)}, bf16[768,128]{1,0:T(8,128)(2,1)}, u32[]{:S(2)}) copy-start(bf16[768,128]{1,0:T(8,128)(2,1)} %param.9) | copy-start | bytes 589828
  6.5 53.3 %all-gather.7.cloned.1.call-start = ((), (), s32[]{:S(2)}) async-start(), calls=%async_computation.2 | async-start | bytes 1769472 | tf_op jit(solution)/shard_map/all_gather | solution.py:10
  7.3 75.1 %all-gather.5.cloned.1.call-start = ((), (), s32[]{:S(2)}) async-start(), calls=%async_computation.1 | async-start | bytes 2621440 | tf_op jit(solution)/shard_map/all_gather | solution.py:23
  10.6 100.6 %all-gather.11.cloned.1.call-start = ((), (), s32[]{:S(2)}) async-start(), calls=%async_computation.4 | async-start | bytes 2359296 | tf_op jit(solution)/shard_map/all_gather | solution.py:34
  36.9 120.5 %all-gather.9.cloned.1.call-start = ((), (), s32[]{:S(2)}) async-start(), calls=%async_computation.3 | async-start | bytes 1769472 | tf_op jit(solution)/shard_map/all_gather | solution.py:10
  37.5 172.1 %reduce-scatter.2.cloned.1.call-start = ((), (), s32[]{:S(2)}) async-start(), calls=%async_computation.5 | async-start | bytes 5242880 | tf_op jit(solution)/shard_map/reduce_scatter | solution.py:16
  82.4 74.9 %copy-start.1 = (bf16[1024,1024]{1,0:T(8,128)(2,1)S(1)}, bf16[1024,1024]{1,0:T(8,128)(2,1)}, u32[]{:S(2)}) copy-start(bf16[1024,1024]{1,0:T(8,128)(2,1)} %all-gather.5.cloned.1.call-done) | copy-start | bytes 6291460
Sparse Core Ops, SparseCore 0:
  9.4 50.3 all-gather.6
  61.4 20.9 all-gather.4
  83.9 27.1 all-gather.10
  113.1 44.1 all-gather.8
  166.6 42.9 reduce-scatter.1
where the time goes:
time: 218 us
  waiting for transfers between devices  159 us (73%)
  blocking collectives  26.2 us (12%)
  matrix products  14.8 us (7%)
  between operations  13.2 us (6%)
  other arithmetic  5.36 us (2%)
    all_gather x2, waiting for transfers between devices, over_all(): lax.all_gather(part, axis, axis=dim, tiled=True)  68.5 us
    reduce_scatter x1, waiting for transfers between devices, summed_rows(): lax.psum_scatter(portion(jnp.int32(0), count), axis, scatter_dimension=0,...  43.1 us
    all_gather x1, blocking collectives, on_device(): own_half = lax.all_gather(down_weight, 'fs', axis=1, tiled=True)  26.2 us
    all_gather x1, waiting for transfers between devices, on_device(): down_whole = lax.all_gather(own_half, 'rep', axis=1, tiled=True)  23.1 us
    all_gather x1, waiting for transfers between devices, on_device(): gathered = lax.all_gather(normed, 'tp', axis=0, tiled=True)  22.5 us
    dot_general x1, matrix products, row_terms(): return jnp.dot(token_block, down_whole, preferred_element_type=jnp.float32)  9.14 us
    dot_general x1, matrix products, add_block(): jnp.dot(columns, row_block, preferred_element_type=jnp.float32)  5.65 us
  transfers between devices with their start and end apart: 5, of which 5 were waited for; matrix products, arithmetic and copies ran while one was open for 4% of the time, Pallas kernels for 0%

commit v1 on v0

--- a/solution.py
+++ b/solution.py
@@ -31,7 +31,7 @@
     up_value = over_all(up_weight, ("rep", "fs"), 0, add_block, zero_sums)
     hidden = (jax.nn.silu(gate_value) * up_value).astype(jnp.bfloat16)
     own_half = lax.all_gather(down_weight, "fs", axis=1, tiled=True)
-    down_whole = lax.all_gather(own_half, "rep", axis=1, tiled=True)
+    down_whole = jnp.concatenate(lax.all_gather(own_half, "rep"), axis=1)
     own_rows = tokens.shape[0]
 
     def row_terms(first_row, row_count):

time: 218 us -> 230 us (1.055)
  waiting for transfers between devices: 159 us -> 176 us
  blocking collectives: 26.2 us -> 21.2 us
    all_gather x2, waiting for transfers between devices: 68.5 us -> 85.3 us  [over_all(): lax.all_gather(part, axis, axis=dim, tiled=True)]
    all_gather x1, blocking collectives: 26.2 us -> 21.2 us  [on_device(): own_half = lax.all_gather(down_weight, 'fs', axis=1, tiled=True)]
where the time goes in v1:
time: 230 us
  waiting for transfers between devices  176 us (77%)
  blocking collectives  21.2 us (9%)
  matrix products  14.8 us (6%)
  between operations  13.2 us (6%)
  other arithmetic  3.27 us (1%)
    all_gather x2, waiting for transfers between devices, over_all(): lax.all_gather(part, axis, axis=dim, tiled=True)  85.3 us
    reduce_scatter x1, waiting for transfers between devices, summed_rows(): lax.psum_scatter(portion(jnp.int32(0), count), axis, scatter_dimension=0,...  43.1 us
    all_gather x1, waiting for transfers between devices, on_device(): down_whole = jnp.concatenate(lax.all_gather(own_half, 'rep'), axis=1)  23.8 us
    all_gather x1, waiting for transfers between devices, on_device(): gathered = lax.all_gather(normed, 'tp', axis=0, tiled=True)  22.5 us
    all_gather x1, blocking collectives, on_device(): own_half = lax.all_gather(down_weight, 'fs', axis=1, tiled=True)  21.2 us
    dot_general x1, matrix products, row_terms(): return jnp.dot(token_block, down_whole, preferred_element_type=jnp.float32)  9.31 us
    dot_general x1, matrix products, add_block(): jnp.dot(columns, row_block, preferred_element_type=jnp.float32)  5.5 us
  transfers between devices with their start and end apart: 5, of which 5 were waited for; matrix products, arithmetic and copies ran while one was open for 4% of the time, Pallas kernels for 0%

profile of v1, /device:TPU:0, one launch (start us, length us, event | category | flops | bytes accessed | tf_op | source)
XLA Modules:
  0.0 230.3 jit_solution(12556468927730539275)
XLA Ops:
  6.5 0.0 copy-start
  6.5 0.0 copy-start.1
  6.5 0.0 all-gather.12.cloned.1.call-start
  6.5 21.2 %all_gather.21 = bf16[768,512]{1,0:T(8,128)(2,1)} all-gather(bf16[768,128]{1,0:T(8,128)(2,1)} %param.9), channel_id=1, replica_groups=mesh['rep'=2,'fs'=4,'tp'=4] {'fs'}, dimensions={1}, use_global_device_ids=true | all-gather | bytes 983040 | tf_op jit(solution)/shard_map/all_gather | solution.py:33
  27.7 0.0 all-gather.12.cloned.1.call-update
  27.8 0.0 all-gather.8.cloned.1.call-start
  27.8 0.7 all-gather.8.cloned.1.call-update
  28.5 0.0 all-gather.6.cloned.1.call-start
  28.6 0.0 copy-done
  28.6 0.2 fusion.1
  28.8 0.0 copy-done.1
  28.8 1.0 fusion.3
  29.7 0.0 all-gather.6.cloned.1.call-update
  29.8 0.0 all-gather.10.cloned.1.call-start
  29.8 0.5 all-gather.10.cloned.1.call-update
  30.3 0.0 reduce-scatter.2.cloned.1.call-start
  30.4 23.8 %all-gather.12.cloned.1.call-done = bf16[1536,512]{1,0:T(8,128)(2,1)} async-done(((bf16[768,512]{1,0:T(8,128)(2,1)}), bf16[1536,512]{1,0:T(8,128)(2,1)}) %all-gather.12.cloned.1.call-update) | async-done | bytes 1572880 | tf_op jit(solution)/shard_map/all_gather | solution.py:34
  54.2 1.7 copy.6
  55.9 44.6 %all-gather.8.cloned.1.call-done = bf16[1024,768]{1,0:T(8,128)(2,1)} async-done(((bf16[128,768]{1,0:T(8,128)(2,1)}), bf16[1024,768]{1,0:T(8,128)(2,1)}) %all-gather.8.cloned.1.call-update) | async-done | bytes 1572880 | tf_op jit(solution)/shard_map/all_gather | solution.py:10
  100.5 22.5 %all-gather.6.cloned.1.call-done = bf16[1024,1024]{1,0:T(8,128)(2,1)} async-done(((bf16[256,1024]{1,0:T(8,128)(2,1)}), bf16[1024,1024]{1,0:T(8,128)(2,1)}) %all-gather.6.cloned.1.call-update) | async-done | bytes 2097168 | tf_op jit(solution)/shard_map/all_gather | solution.py:23
  123.0 5.5 %fusion.5 = f32[1024,768]{1,0:T(8,128)} fusion(bf16[1024,1024]{1,0:T(8,128)(2,1)} %all-gather.6.cloned.1.call-done, bf16[1024,768]{1,0:T(8,128)(2,1)} %all-gather.8.cloned.1.call-done), kind=kOutput, calls=%fused_computation.9 | convolution fusion | flops 1610612736 | bytes 6815744 | tf_op jit(solution)/shard_map/dot_general | solution.py:28
  128.5 40.7 %all-gather.10.cloned.1.call-done = bf16[1024,768]{1,0:T(8,128)(2,1)} async-done(((bf16[128,768]{1,0:T(8,128)(2,1)}), bf16[1024,768]{1,0:T(8,128)(2,1)}) %all-gather.10.cloned.1.call-update) | async-done | bytes 1572880 | tf_op jit(solution)/shard_map/all_gather | solution.py:10
  169.2 9.3 %fusion = f32[1024,1024]{1,0:T(8,128)} fusion(bf16[768,1024]{0,1:T(8,128)(2,1)S(1)} %bitcast.10, f32[1024,768]{1,0:T(8,128)} %fusion.5, bf16[1024,1024]{1,0:T(8,128)(2,1)} %all-gather.6.cloned.1.call-done, bf16[1024,768]{1,0:T(8,128)(2,1)} %all-gather.10.cloned.1.call-done), kind=kOutput, calls=%fused_computation.1 | convolution fusion | flops 3225944064 | bytes 12582912 | tf_op jit(solution)/shard_map/dot_general | solution.py:39
  178.5 0.0 reduce-scatter.2.cloned.1.call-update
  178.6 43.1 %reduce-scatter.2.cloned.1.call-done = f32[256,1024]{1,0:T(8,128)} async-done(((f32[1024,1024]{1,0:T(8,128)}), f32[256,1024]{1,0:T(8,128)}) %reduce-scatter.2.cloned.1.call-update) | async-done | bytes 1048592 | tf_op jit(solution)/shard_map/reduce_scatter | solution.py:16
  221.7 2.1 convert_element_type.15
  (1 shorter events, 0.0 us)
Async XLA Ops:
  6.5 22.0 %copy-start = (bf16[256,1024]{1,0:T(8,128)(2,1)S(1)}, bf16[256,1024]{1,0:T(8,128)(2,1)}, u32[]{:S(2)}) copy-start(bf16[256,1024]{1,0:T(8,128)(2,1)} %param.5) | copy-start | bytes 1572868
  6.5 22.2 %copy-start.1 = (f32[1024]{0:T(1024)S(1)}, f32[1024]{0:T(1024)}, u32[]{:S(2)}) copy-start(f32[1024]{0:T(1024)} %param.6) | copy-start | bytes 12292
  6.5 47.6 %all-gather.12.cloned.1.call-start = ((), (), s32[]{:S(2)}) async-start(), calls=%async_computation.5 | async-start | bytes 2359296 | tf_op jit(solution)/shard_map/all_gather | solution.py:34
  27.8 72.8 %all-gather.8.cloned.1.call-start = ((), (), s32[]{:S(2)}) async-start(), calls=%async_computation.2 | async-start | bytes 1769472 | tf_op jit(solution)/shard_map/all_gather | solution.py:10
  28.5 94.5 %all-gather.6.cloned.1.call-start = ((), (), s32[]{:S(2)}) async-start(), calls=%async_computation.1 | async-start | bytes 2621440 | tf_op jit(solution)/shard_map/all_gather | solution.py:23
  29.8 139.4 %all-gather.10.cloned.1.call-start = ((), (), s32[]{:S(2)}) async-start(), calls=%async_computation.3 | async-start | bytes 1769472 | tf_op jit(solution)/shard_map/all_gather | solution.py:10
  30.3 191.3 %reduce-scatter.2.cloned.1.call-start = ((), (), s32[]{:S(2)}) async-start(), calls=%async_computation.4 | async-start | bytes 5242880 | tf_op jit(solution)/shard_map/reduce_scatter | solution.py:16
Sparse Core Ops, SparseCore 0:
  27.9 26.2 all-gather.11
  56.3 44.1 all-gather.7
  102.1 20.9 all-gather.5
  125.0 44.1 all-gather.9
  178.7 42.9 reduce-scatter.1
